TPU v7x, 32 devices: a whole 2x2x4 slice. The times are simulated.
32 devices in a mesh: fs: 4 (over z), tp: 8 (over y, x, core).
Axes of the slice: x: 2, y: 2, z: 4, core: 2. Of those that a mesh axis runs over, the one named last changes fastest.
Arguments:
- block_in: bfloat16 [4096, 2304], P('fs'), may hold values from -6 to 6
- out_cot: bfloat16 [4096, 2304], P('fs'), may hold values from -6 to 6
- gated_out: bfloat16 [4096, 4608], P('fs', 'tp'), may hold values from -6 to 6
- gate_cot: bfloat16 [4096, 4608], P('fs', 'tp'), may hold values from -6 to 6
- factor_out: bfloat16 [2304, 192], P('fs'), may hold values from -0.104166667 to 0.104166667
- factor_z: bfloat16 [2304, 192], P('fs'), may hold values from -0.104166667 to 0.104166667
- weight_out: float32 [4608, 2304], P('tp', 'fs'), may hold values from -0.09375 to 0.09375
- weight_z: float32 [2304, 4608], P('fs', 'tp'), may hold values from -0.125 to 0.125
- first_out: float32 [4608, 192], P('tp', 'fs'), may hold values from -512 to 512
- second_out: float32 [4608, 192], P('tp', 'fs'), may hold values from 819.2 to 20480
- first_z: float32 [192, 4608], P('fs', 'tp'), may hold values from -512 to 512
- second_z: float32 [192, 4608], P('fs', 'tp'), may hold values from 819.2 to 20480
Outputs:
- step_out: float32 [4608, 2304], P('tp', 'fs')
- step_z: float32 [2304, 4608], P('fs', 'tp')
- new_first_out: float32 [4608, 192], P('tp', 'fs')
- new_second_out: float32 [4608, 192], P('tp', 'fs')
- new_first_z: float32 [192, 4608], P('fs', 'tp')
- new_second_z: float32 [192, 4608], P('fs', 'tp')
- copy_out: bfloat16 [4608, 2304], P('tp')
- copy_z: bfloat16 [2304, 4608], P(None, 'tp')
All inputs are finite; a program needn't handle non-finite values.
Results may differ from a plain program's by a relative error of at most 0.0018.
Values may be sent and summed in bfloat16 or wider, within the bound.
A program may use at most 64 MiB of HBM per device.

v0:
```python
import functools

import jax
import jax.numpy as jnp
from jax import lax
from jax.experimental import pallas as pl
from jax.experimental.pallas import tpu as pltpu
from jax.sharding import PartitionSpec as P

beta_first = 0.8
beta_second = 0.9
adam_eps = 1e-08
norm_eps = 1e-06
rate = 0.005

MESH = pl.DeviceIdType.MESH
VMEM = pl.BlockSpec(memory_space=pltpu.VMEM)
PARTS = 4


def remote(src, dst, send, recv, **where):
    return pltpu.make_async_remote_copy(
        src_ref=src, dst_ref=dst, send_sem=send, recv_sem=recv, device_id=where, device_id_type=MESH
    )


def gather_kernel(fs, factor, full, send_z, recv_z, send_x, recv_x, send_c, recv_c, send_d, recv_d):
    me, mine = lax.axis_index("fs"), lax.axis_index("tp")
    part = lax.rem(mine, PARTS)
    far = mine + 2 - 4 * lax.rem(mine // 2, 2)
    near = mine + 1 - 2 * lax.rem(mine, 2)
    far_part = lax.rem(far, PARTS)
    barrier = pltpu.get_barrier_semaphore()
    for d in range(1, fs):
        pl.semaphore_signal(barrier, inc=1, device_id={"fs": lax.rem(me + d, fs)}, device_id_type=MESH)
    for other in (far, near):
        pl.semaphore_signal(barrier, inc=1, device_id={"tp": other}, device_id_type=MESH)
    pl.semaphore_wait(barrier, fs + 1)

    first, second, third, fourth = [], [], [], []
    for d in range(1, fs):
        copy = remote(
            factor.at[part], full.at[me, part], send_z.at[d - 1], recv_z.at[d - 1], fs=lax.rem(me + d, fs)
        )
        copy.start()
        first.append(copy)
    full[me] = factor[...]
    for d in range(1, fs):
        src = lax.rem(me - d + fs, fs)
        first[d - 1].wait_recv()
        block = full.at[src, part]
        copy = remote(block, block, send_x.at[d - 1], recv_x.at[d - 1], tp=far)
        copy.start()
        second.append(copy)
        copy = remote(block, block, send_c.at[d - 1], recv_c.at[d - 1], tp=near)
        copy.start()
        third.append(copy)
    for d in range(1, fs):
        src = lax.rem(me - d + fs, fs)
        second[d - 1].wait_recv()
        block = full.at[src, far_part]
        copy = remote(block, block, send_d.at[d - 1], recv_d.at[d - 1], tp=near)
        copy.start()
        fourth.append(copy)
    for copy in third + fourth:
        copy.wait_recv()
    for copy in first + second + third + fourth:
        copy.wait_send()


def gather_factors(fs, factors):
    parts, rows, columns = factors.shape
    dma = pltpu.SemaphoreType.DMA((fs - 1,))
    return pl.pallas_call(
        functools.partial(gather_kernel, fs),
        out_shape=jax.ShapeDtypeStruct((fs, parts, rows, columns), factors.dtype),
        in_specs=[VMEM],
        out_specs=VMEM,
        scratch_shapes=[dma] * 8,
        compiler_params=pltpu.CompilerParams(collective_id=0, has_side_effects=True),
        cost_estimate=pl.CostEstimate(flops=0, bytes_accessed=30_000_000, transcendentals=0),
    )(factors)


def reduce_kernel(
    fs, tp, term_out, term_z, first, second, full_out, full_z,
    new_first, new_second, dirs, high, low, total,
    arrived, partial, received, send_r, recv_r, send_g, recv_g, send_t, recv_t,
):
    me, mine = lax.axis_index("fs"), lax.axis_index("tp")
    terms = (term_out, term_z)
    fulls = (full_out, full_z)
    rank = first.shape[1]
    barrier = pltpu.get_barrier_semaphore()
    for d in range(1, fs):
        pl.semaphore_signal(barrier, inc=1, device_id={"fs": lax.rem(me + d, fs)}, device_id_type=MESH)
    for d in range(1, tp):
        pl.semaphore_signal(barrier, inc=1, device_id={"tp": lax.rem(mine + d, tp)}, device_id_type=MESH)
    pl.semaphore_wait(barrier, fs + tp - 2)

    sums = []
    for m in range(2):
        for d in range(1, fs):
            peer = lax.rem(me + d, fs)
            copy = remote(
                terms[m].at[peer], arrived.at[m, d - 1], send_r.at[m, d - 1], recv_r.at[m, d - 1], fs=peer
            )
            copy.start()
            sums.append(copy)
    gathers = []
    for m in range(2):
        gradient = terms[m][me]
        for d in range(1, fs):
            sums[m * (fs - 1) + d - 1].wait_recv()
            gradient = gradient + arrived[m, d - 1]
        moment = beta_first * first[m] + (1.0 - beta_first) * gradient
        square = beta_second * second[m] + (1.0 - beta_second) * gradient * gradient
        new_first[m] = moment
        new_second[m] = square
        dirs[m, me] = moment / (jnp.sqrt(square) + adam_eps)
        for d in range(1, fs):
            block = dirs.at[m, me]
            copy = remote(
                block, block, send_g.at[m, d - 1], recv_g.at[m, d - 1], fs=lax.rem(me + d, fs)
            )
            copy.start()
            gathers.append(copy)
    squares = []
    for m in range(2):
        for d in range(1, fs):
            gathers[m * (fs - 1) + d - 1].wait_recv()
        whole = jnp.concatenate([dirs[m, s] for s in range(fs)], axis=0)
        high_part = whole.astype(jnp.bfloat16)
        low_part = (whole - high_part.astype(jnp.float32)).astype(jnp.bfloat16)
        high[m] = high_part
        low[m] = low_part

        def body(s, acc):
            rows = fulls[m][s]
            update = jnp.dot(rows, high[m], preferred_element_type=jnp.float32)
            update = update + jnp.dot(rows, low[m], preferred_element_type=jnp.float32)
            return acc + jnp.sum(update * update, axis=0, keepdims=True)

        acc = lax.fori_loop(0, fs, body, jnp.zeros((1, whole.shape[1]), jnp.float32))
        squares.append(jnp.sum(acc))
    row = lax.broadcasted_iota(jnp.int32, partial.shape, 0)
    partial[...] = jnp.where(row == 0, squares[0], squares[1])
    totals = []
    for d in range(1, tp):
        copy = remote(
            partial, received.at[d - 1], send_t.at[d - 1], recv_t.at[d - 1], tp=lax.rem(mine + d, tp)
        )
        copy.start()
        totals.append(copy)
    result = partial[...]
    for d in range(1, tp):
        totals[d - 1].wait_recv()
        result = result + received[d - 1]
    total[...] = result
    for copy in sums + gathers + totals:
        copy.wait_send()


def reduce_moments(fs, tp, term_out, term_z, first, second, full_out, full_z):
    _, rank, inner = first.shape
    dma = pltpu.SemaphoreType.DMA
    shape = jax.ShapeDtypeStruct
    f32, bf16 = jnp.float32, jnp.bfloat16
    return pl.pallas_call(
        functools.partial(reduce_kernel, fs, tp),
        out_shape=(
            shape(first.shape, f32),
            shape(first.shape, f32),
            shape((2, fs, rank, inner), f32),
            shape((2, fs * rank, inner), bf16),
            shape((2, fs * rank, inner), bf16),
            shape((8, 128), f32),
        ),
        in_specs=[VMEM] * 6,
        out_specs=[VMEM] * 6,
        scratch_shapes=[
            pltpu.VMEM((2, fs - 1, rank, inner), f32),
            pltpu.VMEM((8, 128), f32),
            pltpu.VMEM((tp - 1, 8, 128), f32),
            dma((2, fs - 1)),
            dma((2, fs - 1)),
            dma((2, fs - 1)),
            dma((2, fs - 1)),
            dma((tp - 1,)),
            dma((tp - 1,)),
        ],
        compiler_params=pltpu.CompilerParams(
            collective_id=1, has_side_effects=True, vmem_limit_bytes=48 * 1024 * 1024
        ),
        cost_estimate=pl.CostEstimate(flops=0, bytes_accessed=100_000_000, transcendentals=0),
    )(term_out, term_z, first, second, full_out, full_z)


def copies_kernel(fs, own_out, own_z, all_out, all_z, kept, send_a, recv_a, send_b, recv_b):
    me = lax.axis_index("fs")
    barrier = pltpu.get_barrier_semaphore()

    @pl.when(me > 0)
    def _():
        pl.semaphore_signal(barrier, inc=1, device_id={"fs": me - 1}, device_id_type=MESH)

    @pl.when(me < fs - 1)
    def _():
        pl.semaphore_signal(barrier, inc=1, device_id={"fs": me + 1}, device_id_type=MESH)

    pl.semaphore_wait(barrier, jnp.minimum(me, 1) + jnp.minimum(fs - 1 - me, 1))

    owns, alls = (own_out, own_z), (all_out, all_z)
    local = [pltpu.make_async_copy(owns[m], alls[m].at[me], kept.at[m]) for m in range(2)]
    for copy in local:
        copy.start()

    def up(m, src, block, step):
        return remote(block, alls[m].at[src], send_a.at[m, step], recv_a.at[m, step], fs=me + 1)

    def down(m, src, block, step):
        return remote(block, alls[m].at[src], send_b.at[m, step], recv_b.at[m, step], fs=me - 1)

    for step in range(fs - 1):
        for m in range(2):
            below, above = me - step, me + step
            held_below = jnp.maximum(below, 0)
            held_above = jnp.minimum(above, fs - 1)
            if step > 0:
                @pl.when(below >= 0)
                def _(m=m, held_below=held_below, step=step):
                    block = alls[m].at[held_below]
                    up(m, held_below, block, step - 1).wait_recv()

                @pl.when(above < fs)
                def _(m=m, held_above=held_above, step=step):
                    block = alls[m].at[held_above]
                    down(m, held_above, block, step - 1).wait_recv()

            @pl.when((below >= 0) & (me < fs - 1))
            def _(m=m, held_below=held_below, step=step):
                block = owns[m] if step == 0 else alls[m].at[held_below]
                up(m, held_below, block, step).start()

            @pl.when((above < fs) & (me > 0))
            def _(m=m, held_above=held_above, step=step):
                block = owns[m] if step == 0 else alls[m].at[held_above]
                down(m, held_above, block, step).start()

    last = fs - 2
    for m in range(2):
        @pl.when(me - last - 1 >= 0)
        def _(m=m):
            up(m, 0, alls[m].at[0], last).wait_recv()

        @pl.when(me + last + 1 < fs)
        def _(m=m):
            down(m, 0, alls[m].at[0], last).wait_recv()

    for step in range(fs - 1):
        for m in range(2):
            @pl.when((me - step >= 0) & (me < fs - 1))
            def _(m=m, step=step):
                up(m, 0, owns[m], step).wait_send()

            @pl.when((me + step < fs) & (me > 0))
            def _(m=m, step=step):
                down(m, 0, owns[m], step).wait_send()
    for copy in local:
        copy.wait()


def gather_copies(fs, own_out, own_z):
    dma = pltpu.SemaphoreType.DMA((2, fs - 1))
    return pl.pallas_call(
        functools.partial(copies_kernel, fs),
        out_shape=tuple(jax.ShapeDtypeStruct((fs,) + own.shape, own.dtype) for own in (own_out, own_z)),
        in_specs=[VMEM] * 2,
        out_specs=[VMEM] * 2,
        scratch_shapes=[pltpu.SemaphoreType.DMA((2,)), dma, dma, dma, dma],
        compiler_params=pltpu.CompilerParams(collective_id=2, has_side_effects=True),
        cost_estimate=pl.CostEstimate(flops=0, bytes_accessed=100_000_000, transcendentals=0),
    )(own_out, own_z)


def split_parts(values):
    high_part = values.astype(jnp.bfloat16)
    low_part = (values - high_part.astype(jnp.float32)).astype(jnp.bfloat16)
    return (high_part, low_part)


def per_device(
    fs, tp,
    block_in, out_cot, gated_out, gate_cot, factor_out, factor_z,
    weight_out, weight_z, first_out, second_out, first_z, second_z,
):
    width, rank = factor_out.shape[0], factor_out.shape[1]
    inner = gated_out.shape[1]
    entries = width * fs * inner * tp

    both = jnp.concatenate([factor_out, factor_z], axis=1).reshape(PARTS, width // PARTS, 2 * rank)
    full = gather_factors(fs, both).reshape(width * fs, 2 * rank)
    full_out, full_z = full[:, :rank], full[:, rank:]

    def term(values, factor, other):
        proj = jnp.dot(values, factor, preferred_element_type=jnp.float32)
        high_part, low_part = split_parts(proj)
        return jnp.dot(high_part.T, other, preferred_element_type=jnp.float32) + jnp.dot(
            low_part.T, other, preferred_element_type=jnp.float32
        )

    term_out = term(out_cot, full_out, gated_out).reshape(fs, rank // fs, inner)
    term_z = term(block_in, full_z, gate_cot).reshape(fs, rank // fs, inner)
    new_first, new_second, _, high, low, total = reduce_moments(
        fs, tp, term_out, term_z,
        jnp.stack([first_out.T, first_z]), jnp.stack([second_out.T, second_z]),
        full_out.reshape(fs, width, rank), full_z.reshape(fs, width, rank),
    )
    scale_out = lax.rsqrt(total[0, 0] / entries + norm_eps)
    scale_z = lax.rsqrt(total[1, 0] / entries + norm_eps)
    pair = jnp.concatenate([high, low], axis=1)

    def twice(factor):
        return jnp.concatenate([factor, factor], axis=1)

    def of_out(factor):
        return lax.dot_general(
            pair[0], twice(factor), (((0,), (1,)), ((), ())), preferred_element_type=jnp.float32
        )

    def of_z(factor):
        return jnp.dot(twice(factor), pair[1], preferred_element_type=jnp.float32)

    step_out = of_out(factor_out) * scale_out
    step_z = of_z(factor_z) * scale_z
    fresh_out = (weight_out - rate * step_out).astype(jnp.bfloat16)
    fresh_z = (weight_z - rate * step_z).astype(jnp.bfloat16)
    copies_out, copies_z = gather_copies(fs, fresh_out, fresh_z)
    copy_out = copies_out.transpose(1, 0, 2).reshape(inner, fs * width)
    copy_z = copies_z.reshape(fs * width, inner)
    return (
        step_out, step_z,
        new_first[0].T, new_second[0].T, new_first[1], new_second[1],
        copy_out, copy_z,
    )


def solution(mesh):
    return jax.shard_map(
        functools.partial(per_device, mesh.shape["fs"], mesh.shape["tp"]),
        mesh=mesh,
        in_specs=(
            P("fs", None),
            P("fs", None),
            P("fs", "tp"),
            P("fs", "tp"),
            P("fs", None),
            P("fs", None),
            P("tp", "fs"),
            P("fs", "tp"),
            P("tp", "fs"),
            P("tp", "fs"),
            P("fs", "tp"),
            P("fs", "tp"),
        ),
        out_specs=(
            P("tp", "fs"),
            P("fs", "tp"),
            P("tp", "fs"),
            P("tp", "fs"),
            P("fs", "tp"),
            P("fs", "tp"),
            P("tp", None),
            P(None, "tp"),
        ),
        check_vma=False,
    )
```

profile of v0, /device:TPU:1, one launch (start us, length us, event | category | flops | bytes accessed | tf_op | source)
XLA Modules:
  0.0 219.3 jit_solution(9607941696244868244)
XLA Ops:
  0.6 0.0 copy-start
  0.6 1.1 pad_maximum_fusion.5.first
  1.7 1.0 pad_maximum_fusion.6.second
  2.7 1.1 pad_maximum_fusion.1
  3.8 1.0 copy.22
  4.8 23.2 %shard_map.179 = bf16[4,4,144,384]{3,2,1,0:T(8,128)(2,1)} custom-call(bf16[4,144,384]{2,1,0:T(8,128)(2,1)} %bitcast.61), custom_call_target="tpu_custom_call" | custom-call | bytes 30000000 | tf_op jit(solution)/shard_map/pallas_call | solution.py:74
  28.0 4.8 %convolution_bitcast_fusion = f32[1024,192]{0,1:T(8,128)S(1)} fusion(bf16[1024,2304]{1,0:T(8,128)(2,1)} %param.12, bf16[2304,384]{1,0:T(8,128)(2,1)} %bitcast.55), kind=kOutput, calls=%fused_computation.4 | convolution fusion | flops 905969664 | bytes 6684672 | tf_op jit(solution)/shard_map/dot_general | solution.py:306
  32.8 0.0 copy-done
  32.8 0.6 fusion.3
  33.4 0.0 copy-start.1
  33.4 0.6 convolution_add_fusion
  34.1 0.8 copy-done.1
  34.9 4.2 %convolution_bitcast_fusion.1 = f32[1024,192]{0,1:T(8,128)S(1)} fusion(bf16[1024,2304]{1,0:T(8,128)(2,1)} %param.13, bf16[2304,384]{1,0:T(8,128)(2,1)S(1)} %bitcast.56), kind=kOutput, calls=%fused_computation.5 | convolution fusion | flops 905969664 | bytes 6684672 | tf_op jit(solution)/shard_map/dot_general | solution.py:306
  39.1 0.0 copy-done.2
  39.1 0.6 fusion.6
  39.7 0.6 convolution_add_fusion.1
  40.3 1.5 fusion.12
  41.8 53.8 %shard_map.180 = (f32[2,48,576]{2,1,0:T(8,128)S(1)}, f32[2,48,576]{2,1,0:T(8,128)S(1)}, f32[2,4,48,576]{3,2,1,0:T(8,128)}, bf16[2,192,576]{2,1,0:T(8,128)(2,1)S(...) custom-call(f32[4,48,576]{2,1,0:T(8,128)S(1)} %bitcast.53, f32[4,48,576]{2,1,0:T(8,128)S(1)} %bitcast.52, ...), custom_call_target="tpu_custom_call" | custom-call | bytes 100000000 | tf_op jit(solution)/shard_map/pallas_call | solution.py:169
  95.7 0.5 fusion.13
  97.6 0.0 copy-start.3
  97.6 0.0 copy-start.5
  97.6 0.1 constant_dynamic-update-slice_fusion
  97.7 0.8 slice_bitcast_fusion.4
  98.5 0.6 copy-done.3
  99.1 0.0 copy-done.5
  99.1 2.0 subtract_convert_fusion
  101.1 0.0 copy-done.4
  101.1 2.0 subtract_convert_fusion.1
  103.1 102.6 %shard_map.181 = (bf16[4,576,576]{2,1,0:T(8,128)(2,1)}, bf16[4,576,576]{2,1,0:T(8,128)(2,1)}) custom-call(bf16[576,576]{1,0:T(8,128)(2,1)} %get-tuple-element.46.own_out, bf16[576,576]{1,0:T(8,128)(2,1)} %get-tuple-element.48.own_z), custom_call_target="tpu_custom_call" | custom-call | bytes 100000000 | tf_op jit(solution)/shard_map/pallas_call | solution.py:275
  205.7 4.7 %copy.23 = bf16[576,4,576]{0,2,1:T(8,128)(2,1)} copy(bf16[576,4,576]{2,0,1:T(8,128)(2,1)} %bitcast.60) | data formatting | bytes 5308416 | tf_op jit(solution)/shard_map/transpose | solution.py:339
  210.4 4.5 %copy.24 = bf16[576,2304]{1,0:T(8,128)(2,1)} copy(bf16[576,2304]{0,1:T(8,128)(2,1)} %bitcast.54) | data formatting | bytes 5308416
  214.8 4.5 %copy.25 = bf16[2304,576]{0,1:T(8,128)(2,1)} copy(bf16[2304,576]{1,0:T(8,128)(2,1)} %bitcast.59) | data formatting | bytes 5308416
  (5 shorter events, 0.1 us)
Async XLA Ops:
  0.6 32.2 %copy-start = (bf16[1024,576]{0,1:T(8,128)(2,1)S(1)}, bf16[1024,576]{0,1:T(8,128)(2,1)}, u32[]{:S(2)}) copy-start(bf16[1024,576]{0,1:T(8,128)(2,1)} %param.15) | copy-start | bytes 3538948
  33.4 1.5 copy-start.1
  34.9 4.2 %copy-start.2 = (bf16[1024,576]{0,1:T(8,128)(2,1)S(1)}, bf16[1024,576]{0,1:T(8,128)(2,1)}, u32[]{:S(2)}) copy-start(bf16[1024,576]{0,1:T(8,128)(2,1)} %param.14) | copy-start | bytes 3538948
  97.6 1.6 copy-start.3
  97.6 1.6 copy-start.5
  99.1 2.0 copy-start.4
  99.1 2.0 copy-start.6
where the time goes:
time: 221 us; the launch traced here: 219 us
  Pallas kernels  180 us (81%)
  local copies, waits for them, and re-layouts  19.1 us (9%)
  matrix products  15.4 us (7%)
  other arithmetic  3.17 us (1%)
    pallas_call x1, Pallas kernels, gather_copies(): pl.pallas_call(functools.partial(copies_kernel, fs), out_shape=tuple((jax...  103 us
    pallas_call x1, Pallas kernels, reduce_moments(): pl.pallas_call(functools.partial(reduce_kernel, fs, tp), out_shape=(shape...  53.8 us
    pallas_call x1, Pallas kernels, gather_factors(): pl.pallas_call(functools.partial(gather_kernel, fs), out_shape=jax.ShapeD...  23.2 us
    unnamed x17, local copies, waits for them, and re-layouts  10.5 us
    dot_general x2, matrix products, term(): proj = jnp.dot(values, factor, preferred_element_type=jnp.float32)  8.99 us
    transpose x1, local copies, waits for them, and re-layouts, per_device(): copy_out = copies_out.transpose(1, 0, 2).reshape(inner, fs * width)  4.68 us

commit v1 on v0

v1 whole, which is shorter than its diff:
```python
import functools
import math

import jax
import jax.numpy as jnp
from jax import lax
from jax.experimental import pallas as pl
from jax.experimental.pallas import tpu as pltpu
from jax.sharding import PartitionSpec as P

beta_first = 0.8
beta_second = 0.9
adam_eps = 1e-08
norm_eps = 1e-06
rate = 0.005

MESH = pl.DeviceIdType.MESH
VMEM = pl.BlockSpec(memory_space=pltpu.VMEM)
ANY = pl.BlockSpec(memory_space=pl.ANY)
PARTS = 8
SPAN = 120.0 * math.log(2.0)
WEIGHT_BOUND = 0.125
DIR_BOUND = 16.0
VALUE_BOUND = 6.0
FACTOR_BOUND = 0.104166667

f32, bf16 = jnp.float32, jnp.bfloat16


def remote(src, dst, send, recv, **where):
    return pltpu.make_async_remote_copy(
        src_ref=src, dst_ref=dst, send_sem=send, recv_sem=recv, device_id=where, device_id_type=MESH
    )


def encode(values, bound, roots):
    size = jnp.abs(values) * (1.0 / bound)
    for _ in range(roots):
        size = jnp.sqrt(size)
    code = jnp.exp(size * (2.0 * SPAN) - SPAN)
    return jnp.where(values < 0.0, -code, code).astype(bf16)


def decode(code, bound, roots):
    code = code.astype(f32)
    size = (jnp.log(jnp.abs(code)) + SPAN) * (0.5 / SPAN)
    for _ in range(roots):
        size = size * size
    size = size * bound
    return jnp.where(code < 0.0, -size, size)


def split(values):
    high = values.astype(bf16)
    return high, (values - high.astype(f32)).astype(bf16)


def nn(a, b):
    return jnp.dot(a, b, preferred_element_type=f32)


def nt(a, b):
    return lax.dot_general(a, b, (((1,), (1,)), ((), ())), preferred_element_type=f32)


def tn(a, b):
    return lax.dot_general(a, b, (((0,), (0,)), ((), ())), preferred_element_type=f32)


def flip(index, bit):
    return index + bit - 2 * bit * lax.rem(index // bit, 2)


def main_kernel(
    fs, tp, chunks, grad_bound,
    out_cot, block_in, gated, gate, factor_out, factor_z, weight_out, weight_z,
    first_out, second_out, first_z, second_z,
    copy_out, copy_z, step_out, step_z, new_first_out, new_second_out, new_first_z, new_second_z,
    tokens_v, inner_v, wo_v, wz_v, wt_v, moments_v,
    full, wall, joined, term, term_code, arrived, dir_code, dir_t, dir_n, update,
    partial, received,
    load, send_f, recv_f, send_p, recv_p, send_u, recv_u, send_d, recv_d,
    send_r, recv_r, send_g, recv_g, send_t, recv_t,
):
    me, mine = lax.axis_index("fs"), lax.axis_index("tp")
    inner, width = weight_out.shape
    rank = factor_out.shape[0]
    share = rank // fs
    tokens = out_cot.shape[0]
    rows = inner // chunks
    entries = float(width * fs * inner * tp)
    part = lax.rem(mine, PARTS)
    piece = 2 * rank // PARTS

    loads = []

    def fetch(src, dst):
        copy = pltpu.make_async_copy(src, dst, load.at[len(loads)])
        copy.start()
        loads.append(copy)
        return copy

    in_factor = [
        fetch(factor_out, full.at[me, pl.ds(0, rank)]),
        fetch(factor_z, full.at[me, pl.ds(rank, rank)]),
    ]
    in_weight = [fetch(weight_out, wo_v), fetch(weight_z, wz_v)]
    in_tokens = [
        (fetch(out_cot, tokens_v.at[0]), fetch(gated, inner_v.at[0])),
        (fetch(block_in, tokens_v.at[1]), fetch(gate, inner_v.at[1])),
    ]
    in_moments = [
        fetch(ref, moments_v.at[i]) for i, ref in enumerate((first_out, first_z, second_out, second_z))
    ]

    barrier = pltpu.get_barrier_semaphore()
    for d in range(1, fs):
        pl.semaphore_signal(barrier, inc=1, device_id={"fs": lax.rem(me + d, fs)}, device_id_type=MESH)
    for d in range(1, tp):
        pl.semaphore_signal(barrier, inc=1, device_id={"tp": lax.rem(mine + d, tp)}, device_id_type=MESH)

    for copy in in_weight:
        copy.wait()
    wt_v[...] = wz_v[...].T

    def pack(r, _):
        at = pl.ds(pl.multiple_of(r * 16, 16), 16)
        pair = jnp.concatenate([wo_v[at, :], wt_v[at, :]], axis=1)
        wall[me, at, :] = encode(pair, WEIGHT_BOUND, 1)
        return 0

    lax.fori_loop(0, inner // 16, pack, 0)
    for copy in in_factor:
        copy.wait()
    pl.semaphore_wait(barrier, fs + tp - 2)

    def piece_of(src, p):
        return full.at[src, pl.ds(pl.multiple_of(p * piece, piece), piece)]

    spread = []
    for d in range(1, fs):
        block = piece_of(me, part)
        copy = remote(block, block, send_f.at[d - 1], recv_f.at[d - 1], fs=lax.rem(me + d, fs))
        copy.start()
        spread.append(copy)

    def chunk_of(src, c):
        return wall.at[src, pl.ds(pl.multiple_of(c * rows, rows), rows)]

    def up(h, c):
        block = chunk_of(jnp.maximum(me - h, 0), c)
        return remote(block, block, send_u.at[h, c], recv_u.at[h, c], fs=jnp.minimum(me + 1, fs - 1))

    def down(h, c):
        block = chunk_of(jnp.minimum(me + h, fs - 1), c)
        return remote(block, block, send_d.at[h, c], recv_d.at[h, c], fs=jnp.maximum(me - 1, 0))

    def start_own(c, _):
        @pl.when(me < fs - 1)
        def _():
            up(0, c).start()

        @pl.when(me > 0)
        def _():
            down(0, c).start()

        return 0

    lax.fori_loop(0, chunks, start_own, 0)

    def pump(h):
        def body(c, _):
            @pl.when((me - h >= 0) & (me < fs - 1))
            def _():
                up(h - 1, c).wait_recv()
                up(h, c).start()

            @pl.when((me + h < fs) & (me > 0))
            def _():
                down(h - 1, c).wait_recv()
                down(h, c).start()

            return 0

        lax.fori_loop(0, chunks, body, 0)

    plane = []

    def pass_on(d, k, p, bit):
        block = piece_of(lax.rem(me - d + fs, fs), p)
        copy = remote(block, block, send_p.at[d - 1, k], recv_p.at[d - 1, k], tp=flip(mine, bit))
        copy.start()
        plane.append(copy)
        return copy

    by_y, by_x = [], []
    for d in range(1, fs):
        spread[d - 1].wait_recv()
        by_y.append(pass_on(d, 0, part, 4))
        by_x.append([pass_on(d, 1, part, 2)])
        pass_on(d, 3, part, 1)
    for d in range(1, fs):
        by_y[d - 1].wait_recv()
        by_x[d - 1].append(pass_on(d, 2, flip(part, 4), 2))
        pass_on(d, 4, flip(part, 4), 1)
    for d in range(1, fs):
        for k, copy in enumerate(by_x[d - 1]):
            copy.wait_recv()
            p = flip(part, 2)
            pass_on(d, 5 + k, p if k == 0 else flip(p, 4), 1)
    waited = [c for c in by_y] + [c for pair in by_x for c in pair]
    for copy in plane:
        if not any(copy is other for other in waited):
            copy.wait_recv()

    block_t = 256 if tokens % 256 == 0 else tokens
    for m in range(2):
        joined[m] = jnp.concatenate(
            [full[s, pl.ds(m * rank, rank), :] for s in range(fs)], axis=1
        )
        for copy in in_tokens[m]:
            copy.wait()

        def project(c, _, m=m):
            at = pl.ds(pl.multiple_of(c * block_t, block_t), block_t)
            high, low = split(nt(joined[m], tokens_v[m, at, :]))
            other = inner_v[m, :, at]
            value = nt(high, other) + nt(low, other)
            term[m] = jnp.where(c == 0, value, term[m] + value)
            return 0

        term[m] = jnp.zeros((rank, inner), f32)
        lax.fori_loop(0, tokens // block_t, project, 0)

    for s in range(fs):
        at = pl.ds(s * share, share)
        term_code[s] = encode(
            jnp.concatenate([term[0, at, :], term[1, at, :]], axis=1), grad_bound, 4
        )
    if fs > 2:
        pump(1)
    sums = []
    for d in range(1, fs):
        peer = lax.rem(me + d, fs)
        copy = remote(term_code.at[peer], arrived.at[d - 1], send_r.at[d - 1], recv_r.at[d - 1], fs=peer)
        copy.start()
        sums.append(copy)
    for copy in in_moments:
        copy.wait()
    own = pl.ds(pl.multiple_of(me * share, share), share)
    gradient = jnp.concatenate([term[0, own, :], term[1, own, :]], axis=1)
    for d in range(1, fs):
        sums[d - 1].wait_recv()
        gradient = gradient + decode(arrived[d - 1], grad_bound, 4)
    first = jnp.concatenate([moments_v[0], moments_v[1]], axis=1)
    second = jnp.concatenate([moments_v[2], moments_v[3]], axis=1)
    moment = beta_first * first + (1.0 - beta_first) * gradient
    square = beta_second * second + (1.0 - beta_second) * gradient * gradient
    dir_code[me] = encode(moment / (jnp.sqrt(square) + adam_eps), DIR_BOUND, 3)
    new_first_out[...] = moment[:, :inner]
    new_first_z[...] = moment[:, inner:]
    new_second_out[...] = square[:, :inner]
    new_second_z[...] = square[:, inner:]
    gathers = []
    for d in range(1, fs):
        block = dir_code.at[me]
        copy = remote(block, block, send_g.at[d - 1], recv_g.at[d - 1], fs=lax.rem(me + d, fs))
        copy.start()
        gathers.append(copy)
    for h in range(2, fs - 1):
        pump(h)
    for copy in gathers:
        copy.wait_recv()

    whole = decode(jnp.concatenate([dir_code[s] for s in range(fs)], axis=0), DIR_BOUND, 3)
    for m in range(2):
        values = whole[:, m * inner:(m + 1) * inner]
        high, low = split(values.T)
        dir_t[m, 0] = high
        dir_t[m, 1] = low
    high, low = split(whole[:, inner:])
    dir_n[0] = high
    dir_n[1] = low

    squares = []
    for m in range(2):
        def grow(c, acc, m=m):
            at = pl.ds(pl.multiple_of(c * rows, rows), rows)
            value = nn(dir_t[m, 0, at, :], joined[m]) + nn(dir_t[m, 1, at, :], joined[m])
            update[m, at, :] = value
            return acc + jnp.sum(value * value, axis=0, keepdims=True)

        acc = lax.fori_loop(0, chunks, grow, jnp.zeros((1, fs * width), f32))
        squares.append(jnp.sum(acc))
    row = lax.broadcasted_iota(jnp.int32, partial.shape, 0)
    partial[...] = jnp.where(row == 0, squares[0], squares[1])
    own_z = full[me, pl.ds(rank, rank), :]
    step_z[...] = tn(own_z, dir_n[0]) + tn(own_z, dir_n[1])
    totals = []
    for d in range(1, tp):
        copy = remote(
            partial, received.at[d - 1], send_t.at[d - 1], recv_t.at[d - 1], tp=lax.rem(mine + d, tp)
        )
        copy.start()
        totals.append(copy)
    own_out = full[me, pl.ds(0, rank), :]
    step_out[...] = nn(dir_t[0, 0], own_out) + nn(dir_t[0, 1], own_out)
    result = partial[...]
    for d in range(1, tp):
        totals[d - 1].wait_recv()
        result = result + received[d - 1]
    scale = lax.rsqrt(result * (1.0 / entries) + norm_eps)
    scale_out, scale_z = scale[0:1, 0:1], scale[1:2, 0:1]
    step_out[...] = step_out[...] * scale_out
    step_z[...] = step_z[...] * scale_z

    def finish(c, _):
        @pl.when(me == fs - 1)
        def _():
            for h in range(fs - 1):
                up(h, c).wait_recv()

        @pl.when(me == 0)
        def _():
            for h in range(fs - 1):
                down(h, c).wait_recv()

        def fresh(r, _):
            at = pl.ds(pl.multiple_of(c * rows + r * 16, 16), 16)
            for m, (dst, size) in enumerate(((copy_out, scale_out), (copy_z, scale_z))):
                code = jnp.concatenate(
                    [wall[s, at, m * width:(m + 1) * width] for s in range(fs)], axis=1
                )
                step = update[m, at, :] * size
                dst[at, :] = (decode(code, WEIGHT_BOUND, 1) - rate * step).astype(bf16)
            return 0

        lax.fori_loop(0, rows // 16, fresh, 0)
        return 0

    lax.fori_loop(0, chunks, finish, 0)

    for h in range(fs - 1):
        def drain(c, _, h=h):
            @pl.when((me - h >= 0) & (me < fs - 1))
            def _():
                up(h, c).wait_send()

            @pl.when((me + h < fs) & (me > 0))
            def _():
                down(h, c).wait_send()

            return 0

        lax.fori_loop(0, chunks, drain, 0)
    for copy in spread + plane + sums + gathers + totals:
        copy.wait_send()


def store_kernel(*refs):
    count = (len(refs) - 1) // 2
    sems = refs[-1]
    copies = [
        pltpu.make_async_copy(refs[i], refs[count + i], sems.at[i]) for i in range(count)
    ]
    for copy in copies:
        copy.start()
    for copy in copies:
        copy.wait()


def per_device(
    fs, tp,
    block_in, out_cot, gated_out, gate_cot, factor_out, factor_z,
    weight_out, weight_z, first_out, second_out, first_z, second_z,
):
    width, rank = factor_out.shape
    tokens, inner = gated_out.shape
    share = rank // fs
    chunks = next(n for n in (6, 3, 2, 1) if inner % (16 * n) == 0)
    grad_bound = 2.0 ** math.ceil(
        math.log2(tokens * VALUE_BOUND * width * fs * VALUE_BOUND * FACTOR_BOUND)
    )
    dma = pltpu.SemaphoreType.DMA
    shape = jax.ShapeDtypeStruct
    moment = shape((share, inner), f32)
    results = (
        shape((inner, fs * width), bf16),
        shape((inner, fs * width), bf16),
        shape((inner, width), f32),
        shape((width, inner), f32),
        moment, moment, moment, moment,
    )
    hops = dma((fs - 1, chunks))
    peers = dma((fs - 1,))
    others = dma((tp - 1,))
    pieces = dma((fs - 1, PARTS - 1))
    made = pl.pallas_call(
        functools.partial(main_kernel, fs, tp, chunks, grad_bound),
        out_shape=results,
        in_specs=[ANY] * 12,
        out_specs=[VMEM] * 8,
        scratch_shapes=[
            pltpu.VMEM((2, tokens, fs * width), bf16),
            pltpu.VMEM((2, inner, tokens), bf16),
            pltpu.VMEM((inner, width), f32),
            pltpu.VMEM((width, inner), f32),
            pltpu.VMEM((inner, width), f32),
            pltpu.VMEM((4, share, inner), f32),
            pltpu.VMEM((fs, 2 * rank, width), bf16),
            pltpu.VMEM((fs, inner, 2 * width), bf16),
            pltpu.VMEM((2, rank, fs * width), bf16),
            pltpu.VMEM((2, rank, inner), f32),
            pltpu.VMEM((fs, share, 2 * inner), bf16),
            pltpu.VMEM((fs - 1, share, 2 * inner), bf16),
            pltpu.VMEM((fs, share, 2 * inner), bf16),
            pltpu.VMEM((2, 2, inner, rank), bf16),
            pltpu.VMEM((2, rank, inner), bf16),
            pltpu.VMEM((2, inner, fs * width), f32),
            pltpu.VMEM((8, 128), f32),
            pltpu.VMEM((tp - 1, 8, 128), f32),
            dma((12,)),
            peers, peers, pieces, pieces, hops, hops, hops, hops,
            peers, peers, peers, peers, others, others,
        ],
        compiler_params=pltpu.CompilerParams(
            collective_id=0, has_side_effects=True, vmem_limit_bytes=52 * 1024 * 1024
        ),
        cost_estimate=pl.CostEstimate(flops=10**10, bytes_accessed=30_000_000, transcendentals=0),
    )(
        out_cot, block_in, gated_out.T, gate_cot.T, factor_out.T, factor_z.T, weight_out, weight_z,
        first_out.T, second_out.T, first_z, second_z,
    )
    kept = pl.pallas_call(
        store_kernel,
        out_shape=results,
        in_specs=[VMEM] * 8,
        out_specs=[ANY] * 8,
        scratch_shapes=[dma((8,))],
        cost_estimate=pl.CostEstimate(flops=10**6, bytes_accessed=20_000_000, transcendentals=0),
    )(*made)
    copy_out, copy_z, step_out, step_z, nf_out, ns_out, nf_z, ns_z = kept
    return step_out, step_z, nf_out.T, ns_out.T, nf_z, ns_z, copy_out, copy_z.T


def solution(mesh):
    return jax.shard_map(
        functools.partial(per_device, mesh.shape["fs"], mesh.shape["tp"]),
        mesh=mesh,
        in_specs=(
            P("fs", None),
            P("fs", None),
            P("fs", "tp"),
            P("fs", "tp"),
            P("fs", None),
            P("fs", None),
            P("tp", "fs"),
            P("fs", "tp"),
            P("tp", "fs"),
            P("tp", "fs"),
            P("fs", "tp"),
            P("fs", "tp"),
        ),
        out_specs=(
            P("tp", "fs"),
            P("fs", "tp"),
            P("tp", "fs"),
            P("tp", "fs"),
            P("fs", "tp"),
            P("fs", "tp"),
            P("tp", None),
            P(None, "tp"),
        ),
        check_vma=False,
    )
```

time: 221 us -> 140 us (0.63)
  Pallas kernels: 180 us -> 130 us
  matrix products: 15.4 us -> 0 us
  local copies, waits for them, and re-layouts: 19.1 us -> 8.07 us
  other arithmetic: 3.17 us -> 0 us
    pallas_call x3 -> x2, Pallas kernels: 180 us -> 130 us  [the longest x1 124 us: per_device(): pl.pallas_call(functools.partial(main_kernel, fs, tp, chunks, grad_bound)...]
    dot_general x8 -> x0, matrix products: 15.4 us -> none  [the longest x2 8.99 us: term(): proj = jnp.dot(values, factor, preferred_element_type=jnp.float32)]
    transpose x1 -> x0, local copies, waits for them, and re-layouts: 4.68 us -> none  [per_device(): copy_out = copies_out.transpose(1, 0, 2).reshape(inner, fs * width)]
    unnamed x17 -> x20, local copies, waits for them, and re-layouts: 10.5 us -> 8.07 us
where the time goes in v1:
time: 140 us; the launch traced here: 139 us
  Pallas kernels  130 us (93%)
  local copies, waits for them, and re-layouts  8.07 us (6%)
    pallas_call x1, Pallas kernels, per_device(): pl.pallas_call(functools.partial(main_kernel, fs, tp, chunks, grad_bound)...  124 us
    unnamed x20, local copies, waits for them, and re-layouts  8.07 us
    pallas_call x1, Pallas kernels, per_device(): pl.pallas_call(store_kernel, out_shape=results, in_specs=[VMEM] * 8, out_...  6.89 us

profile of v1, /device:TPU:1, one launch (start us, length us, event | category | flops | bytes accessed | tf_op | source)
XLA Modules:
  0.0 139.2 jit_solution(5278550816923428305)
XLA Ops:
  0.6 0.0 copy-start.4
  0.6 0.9 copy-done.4
  1.6 0.0 copy-start.5
  1.6 0.9 copy-done.5
  2.5 0.0 copy-start.6
  2.5 0.9 copy-done.6
  3.4 0.0 copy-start.7
  3.4 0.9 copy-done.7
  4.3 0.0 copy-start.8
  4.3 0.9 copy-done.8
  5.2 0.0 copy-start.9
  5.2 0.9 copy-done.9
  6.1 123.6 %shard_map.179 = (bf16[576,2304]{1,0:T(8,128)(2,1)}, bf16[576,2304]{1,0:T(8,128)(2,1)}, f32[576,576]{1,0:T(8,128)}, f32[576,576]{1,0:T(8,128)}, f32[48,576]{1,0:...) custom-call(bf16[1024,2304]{1,0:T(8,128)(2,1)} %out_cot.1, ...), custom_call_target="tpu_custom_call" | custom-call | flops 10000000000 | bytes 30000000 | tf_op jit(solution)/shard_map/pallas_call | solution.py:398
  129.7 0.0 copy-start
  129.7 0.6 copy-done
  130.4 0.0 copy-start.1
  130.4 0.6 copy-done.1
  131.0 0.0 copy-start.2
  131.0 0.6 copy-done.2
  131.7 0.0 copy-start.3
  131.7 0.6 copy-done.3
  132.3 6.9 %shard_map.180 = (bf16[576,2304]{1,0:T(8,128)(2,1)}, bf16[576,2304]{1,0:T(8,128)(2,1)}, f32[576,576]{1,0:T(8,128)}, f32[576,576]{1,0:T(8,128)}, f32[48,576]{1,0:...) custom-call(bf16[576,2304]{1,0:T(8,128)(2,1)} %get-tuple-element.24.refs_0_, ...), custom_call_target="tpu_custom_call" | custom-call | flops 1000000 | bytes 20000000 | tf_op jit(solution)/shard_map/pallas_call | solution.py:434
Async XLA Ops:
  0.6 0.9 copy-start.4
  1.6 0.9 copy-start.5
  2.5 0.9 copy-start.6
  3.4 0.9 copy-start.7
  4.3 0.9 copy-start.8
  5.2 0.9 copy-start.9
  129.7 0.7 copy-start
  130.4 0.7 copy-start.1
  131.0 0.6 copy-start.2
  131.7 0.7 copy-start.3

commit v2 on v1

--- a/solution.py
+++ b/solution.py
@@ -77,7 +77,7 @@
     first_out, second_out, first_z, second_z,
     copy_out, copy_z, step_out, step_z, new_first_out, new_second_out, new_first_z, new_second_z,
     tokens_v, inner_v, wo_v, wz_v, wt_v, moments_v,
-    full, wall, joined, term, term_code, arrived, dir_code, dir_t, dir_n, update,
+    full, wall, joined, term, rise_out, rise_in, fall_out, fall_in, sum_v, dir_code, dir_t, dir_n, update,
     partial, received,
     load, send_f, recv_f, send_p, recv_p, send_u, recv_u, send_d, recv_d,
     send_r, recv_r, send_g, recv_g, send_t, recv_t,
@@ -105,6 +105,28 @@
         fetch(factor_z, full.at[me, pl.ds(rank, rank)]),
     ]
     in_weight = [fetch(weight_out, wo_v), fetch(weight_z, wz_v)]
+
+    barrier = pltpu.get_barrier_semaphore()
+    for d in range(1, fs):
+        pl.semaphore_signal(barrier, inc=1, device_id={"fs": lax.rem(me + d, fs)}, device_id_type=MESH)
+    for d in range(1, tp):
+        pl.semaphore_signal(barrier, inc=1, device_id={"tp": lax.rem(mine + d, tp)}, device_id_type=MESH)
+    for copy in in_factor:
+        copy.wait()
+    pl.semaphore_wait(barrier, fs + tp - 2)
+
+    def piece_of(src, p):
+        return full.at[src, pl.ds(pl.multiple_of(p * piece, piece), piece)]
+
+    spread = []
+    for d in range(1, fs):
+        block = piece_of(me, part)
+        copy = remote(block, block, send_f.at[d - 1], recv_f.at[d - 1], fs=lax.rem(me + d, fs))
+        copy.start()
+        spread.append(copy)
+
+    for copy in in_weight:
+        copy.wait()
     in_tokens = [
         (fetch(out_cot, tokens_v.at[0]), fetch(gated, inner_v.at[0])),
         (fetch(block_in, tokens_v.at[1]), fetch(gate, inner_v.at[1])),
@@ -112,37 +134,7 @@
     in_moments = [
         fetch(ref, moments_v.at[i]) for i, ref in enumerate((first_out, first_z, second_out, second_z))
     ]
-
-    barrier = pltpu.get_barrier_semaphore()
-    for d in range(1, fs):
-        pl.semaphore_signal(barrier, inc=1, device_id={"fs": lax.rem(me + d, fs)}, device_id_type=MESH)
-    for d in range(1, tp):
-        pl.semaphore_signal(barrier, inc=1, device_id={"tp": lax.rem(mine + d, tp)}, device_id_type=MESH)
-
-    for copy in in_weight:
-        copy.wait()
     wt_v[...] = wz_v[...].T
-
-    def pack(r, _):
-        at = pl.ds(pl.multiple_of(r * 16, 16), 16)
-        pair = jnp.concatenate([wo_v[at, :], wt_v[at, :]], axis=1)
-        wall[me, at, :] = encode(pair, WEIGHT_BOUND, 1)
-        return 0
-
-    lax.fori_loop(0, inner // 16, pack, 0)
-    for copy in in_factor:
-        copy.wait()
-    pl.semaphore_wait(barrier, fs + tp - 2)
-
-    def piece_of(src, p):
-        return full.at[src, pl.ds(pl.multiple_of(p * piece, piece), piece)]
-
-    spread = []
-    for d in range(1, fs):
-        block = piece_of(me, part)
-        copy = remote(block, block, send_f.at[d - 1], recv_f.at[d - 1], fs=lax.rem(me + d, fs))
-        copy.start()
-        spread.append(copy)
 
     def chunk_of(src, c):
         return wall.at[src, pl.ds(pl.multiple_of(c * rows, rows), rows)]
@@ -155,7 +147,7 @@
         block = chunk_of(jnp.minimum(me + h, fs - 1), c)
         return remote(block, block, send_d.at[h, c], recv_d.at[h, c], fs=jnp.maximum(me - 1, 0))
 
-    def start_own(c, _):
+    def start_own(c):
         @pl.when(me < fs - 1)
         def _():
             up(0, c).start()
@@ -164,25 +156,35 @@
         def _():
             down(0, c).start()
 
+    def pack(c, _):
+        at = pl.ds(pl.multiple_of(c * rows, rows), rows)
+        pair = jnp.concatenate([wo_v[at, :], wt_v[at, :]], axis=1)
+        wall[me, at, :] = encode(pair, WEIGHT_BOUND, 1)
+
+        @pl.when(c > 0)
+        def _():
+            start_own(c - 1)
+
         return 0
 
-    lax.fori_loop(0, chunks, start_own, 0)
-
-    def pump(h):
+    lax.fori_loop(0, chunks, pack, 0)
+    start_own(chunks - 1)
+
+    def pump(h, low, high, rising=True, falling=True):
         def body(c, _):
-            @pl.when((me - h >= 0) & (me < fs - 1))
+            @pl.when((me - h >= 0) & (me < fs - 1) & rising)
             def _():
                 up(h - 1, c).wait_recv()
                 up(h, c).start()
 
-            @pl.when((me + h < fs) & (me > 0))
+            @pl.when((me + h < fs) & (me > 0) & falling)
             def _():
                 down(h - 1, c).wait_recv()
                 down(h, c).start()
 
             return 0
 
-        lax.fori_loop(0, chunks, body, 0)
+        lax.fori_loop(low, high, body, 0)
 
     plane = []
 
@@ -232,26 +234,58 @@
         term[m] = jnp.zeros((rank, inner), f32)
         lax.fori_loop(0, tokens // block_t, project, 0)
 
-    for s in range(fs):
-        at = pl.ds(s * share, share)
-        term_code[s] = encode(
-            jnp.concatenate([term[0, at, :], term[1, at, :]], axis=1), grad_bound, 4
+    half = chunks // 2 + 1
+    upper = me * 2 >= fs
+    lower = me * 2 < fs
+    if fs > 2:
+        pump(1, 0, half, upper, lower)
+
+    def rise(t):
+        return remote(
+            rise_out.at[t - 1], rise_in.at[t - 1], send_r.at[0, t - 1], recv_r.at[0, t - 1],
+            fs=jnp.minimum(me + 1, fs - 1),
         )
-    if fs > 2:
-        pump(1)
-    sums = []
-    for d in range(1, fs):
-        peer = lax.rem(me + d, fs)
-        copy = remote(term_code.at[peer], arrived.at[d - 1], send_r.at[d - 1], recv_r.at[d - 1], fs=peer)
-        copy.start()
-        sums.append(copy)
+
+    def fall(t):
+        return remote(
+            fall_out.at[t], fall_in.at[t], send_r.at[1, t], recv_r.at[1, t], fs=jnp.maximum(me - 1, 0)
+        )
+
+    def link(t, first_one, made, move, out, came, slot):
+        at = pl.ds(t * share, share)
+
+        @pl.when(first_one)
+        def _():
+            out[slot] = encode(jnp.concatenate([term[0, at, :], term[1, at, :]], axis=1), grad_bound, 4)
+            move(t).start()
+
+        @pl.when(made)
+        def _():
+            move(t).wait_recv()
+            value = jnp.concatenate([term[0, at, :], term[1, at, :]], axis=1)
+            out[slot] = encode(value + decode(came[slot], grad_bound, 4), grad_bound, 4)
+            move(t).start()
+
+    for k in range(fs - 1):
+        t = fs - 1 - k
+        link(t, me == 0, (me > 0) & (me < t), rise, rise_out, rise_in, t - 1)
+        link(k, me == fs - 1, (me < fs - 1) & (me > k), fall, fall_out, fall_in, k)
     for copy in in_moments:
         copy.wait()
     own = pl.ds(pl.multiple_of(me * share, share), share)
-    gradient = jnp.concatenate([term[0, own, :], term[1, own, :]], axis=1)
-    for d in range(1, fs):
-        sums[d - 1].wait_recv()
-        gradient = gradient + decode(arrived[d - 1], grad_bound, 4)
+    sum_v[...] = jnp.concatenate([term[0, own, :], term[1, own, :]], axis=1)
+
+    @pl.when(me > 0)
+    def _():
+        rise(me).wait_recv()
+        sum_v[...] += decode(rise_in[me - 1], grad_bound, 4)
+
+    @pl.when(me < fs - 1)
+    def _():
+        fall(me).wait_recv()
+        sum_v[...] += decode(fall_in[me], grad_bound, 4)
+
+    gradient = sum_v[...]
     first = jnp.concatenate([moments_v[0], moments_v[1]], axis=1)
     second = jnp.concatenate([moments_v[2], moments_v[3]], axis=1)
     moment = beta_first * first + (1.0 - beta_first) * gradient
@@ -267,8 +301,12 @@
         copy = remote(block, block, send_g.at[d - 1], recv_g.at[d - 1], fs=lax.rem(me + d, fs))
         copy.start()
         gathers.append(copy)
-    for h in range(2, fs - 1):
-        pump(h)
+    if fs > 2:
+        pump(1, half, chunks, upper, lower)
+        pump(1, 0, chunks, lower, upper)
+    few = chunks // 6
+    if fs > 3:
+        pump(2, 0, few)
     for copy in gathers:
         copy.wait_recv()
 
@@ -282,15 +320,16 @@
     dir_n[0] = high
     dir_n[1] = low
 
+    tall = inner // 3 if inner % 48 == 0 else inner
     squares = []
     for m in range(2):
         def grow(c, acc, m=m):
-            at = pl.ds(pl.multiple_of(c * rows, rows), rows)
+            at = pl.ds(pl.multiple_of(c * tall, tall), tall)
             value = nn(dir_t[m, 0, at, :], joined[m]) + nn(dir_t[m, 1, at, :], joined[m])
             update[m, at, :] = value
             return acc + jnp.sum(value * value, axis=0, keepdims=True)
 
-        acc = lax.fori_loop(0, chunks, grow, jnp.zeros((1, fs * width), f32))
+        acc = lax.fori_loop(0, inner // tall, grow, jnp.zeros((1, fs * width), f32))
         squares.append(jnp.sum(acc))
     row = lax.broadcasted_iota(jnp.int32, partial.shape, 0)
     partial[...] = jnp.where(row == 0, squares[0], squares[1])
@@ -305,6 +344,10 @@
         totals.append(copy)
     own_out = full[me, pl.ds(0, rank), :]
     step_out[...] = nn(dir_t[0, 0], own_out) + nn(dir_t[0, 1], own_out)
+    if fs > 3:
+        pump(2, few, chunks)
+    for h in range(3, fs - 1):
+        pump(h, 0, chunks)
     result = partial[...]
     for d in range(1, tp):
         totals[d - 1].wait_recv()
@@ -353,7 +396,18 @@
             return 0
 
         lax.fori_loop(0, chunks, drain, 0)
-    for copy in spread + plane + sums + gathers + totals:
+    for k in range(fs - 1):
+        t = fs - 1 - k
+
+        @pl.when(me < t)
+        def _(t=t):
+            rise(t).wait_send()
+
+        @pl.when(me > k)
+        def _(k=k):
+            fall(k).wait_send()
+
+    for copy in spread + plane + gathers + totals:
         copy.wait_send()
 
 
@@ -377,7 +431,7 @@
     width, rank = factor_out.shape
     tokens, inner = gated_out.shape
     share = rank // fs
-    chunks = next(n for n in (6, 3, 2, 1) if inner % (16 * n) == 0)
+    chunks = next(n for n in (12, 6, 3, 2, 1) if inner % (16 * n) == 0)
     grad_bound = 2.0 ** math.ceil(
         math.log2(tokens * VALUE_BOUND * width * fs * VALUE_BOUND * FACTOR_BOUND)
     )
@@ -393,11 +447,12 @@
     )
     hops = dma((fs - 1, chunks))
     peers = dma((fs - 1,))
+    chain = dma((2, fs - 1))
     others = dma((tp - 1,))
     pieces = dma((fs - 1, PARTS - 1))
     made = pl.pallas_call(
         functools.partial(main_kernel, fs, tp, chunks, grad_bound),
-        out_shape=results,
+        out_shape=tuple(pltpu.VMEM(r.shape, r.dtype) for r in results),
         in_specs=[ANY] * 12,
         out_specs=[VMEM] * 8,
         scratch_shapes=[
@@ -411,8 +466,11 @@
             pltpu.VMEM((fs, inner, 2 * width), bf16),
             pltpu.VMEM((2, rank, fs * width), bf16),
             pltpu.VMEM((2, rank, inner), f32),
-            pltpu.VMEM((fs, share, 2 * inner), bf16),
             pltpu.VMEM((fs - 1, share, 2 * inner), bf16),
+            pltpu.VMEM((fs - 1, share, 2 * inner), bf16),
+            pltpu.VMEM((fs - 1, share, 2 * inner), bf16),
+            pltpu.VMEM((fs - 1, share, 2 * inner), bf16),
+            pltpu.VMEM((share, 2 * inner), f32),
             pltpu.VMEM((fs, share, 2 * inner), bf16),
             pltpu.VMEM((2, 2, inner, rank), bf16),
             pltpu.VMEM((2, rank, inner), bf16),
@@ -421,24 +479,25 @@
             pltpu.VMEM((tp - 1, 8, 128), f32),
             dma((12,)),
             peers, peers, pieces, pieces, hops, hops, hops, hops,
-            peers, peers, peers, peers, others, others,
+            chain, chain, peers, peers, others, others,
         ],
         compiler_params=pltpu.CompilerParams(
-            collective_id=0, has_side_effects=True, vmem_limit_bytes=52 * 1024 * 1024
+            collective_id=0, has_side_effects=True, vmem_limit_bytes=48 * 1024 * 1024
         ),
         cost_estimate=pl.CostEstimate(flops=10**10, bytes_accessed=30_000_000, transcendentals=0),
-    )(
+    )(*[pltpu.with_memory_space_constraint(v, pltpu.HBM) for v in (
         out_cot, block_in, gated_out.T, gate_cot.T, factor_out.T, factor_z.T, weight_out, weight_z,
         first_out.T, second_out.T, first_z, second_z,
-    )
+    )])
     kept = pl.pallas_call(
         store_kernel,
         out_shape=results,
         in_specs=[VMEM] * 8,
         out_specs=[ANY] * 8,
         scratch_shapes=[dma((8,))],
+        compiler_params=pltpu.CompilerParams(vmem_limit_bytes=1024 * 1024),
         cost_estimate=pl.CostEstimate(flops=10**6, bytes_accessed=20_000_000, transcendentals=0),
-    )(*made)
+    )(*[pltpu.with_memory_space_constraint(v, pltpu.VMEM) for v in made])
     copy_out, copy_z, step_out, step_z, nf_out, ns_out, nf_z, ns_z = kept
     return step_out, step_z, nf_out.T, ns_out.T, nf_z, ns_z, copy_out, copy_z.T
 

time: 140 us -> 113 us (0.81); the launches traced: 139 us -> 111 us
  Pallas kernels: 130 us -> 110 us
  local copies, waits for them, and re-layouts: 8.07 us -> 0 us
    pallas_call x1, Pallas kernels: 124 us -> 106 us  [per_device(): pl.pallas_call(functools.partial(main_kernel, fs, tp, chunks, grad_bound)...]
    unnamed x20 -> x0, local copies, waits for them, and re-layouts: 8.07 us -> none
    pallas_call x1, Pallas kernels: 6.89 us -> 3.47 us  [per_device(): pl.pallas_call(store_kernel, out_shape=results, in_specs=[VMEM] * 8, out_...]
where the time goes in v2:
time: 113 us; the launch traced here: 111 us
  Pallas kernels  110 us (97%)
    pallas_call x1, Pallas kernels, per_device(): pl.pallas_call(functools.partial(main_kernel, fs, tp, chunks, grad_bound)...  106 us
    pallas_call x1, Pallas kernels, per_device(): pl.pallas_call(store_kernel, out_shape=results, in_specs=[VMEM] * 8, out_...  3.47 us

profile of v2, /device:TPU:1, one launch (start us, length us, event | category | flops | bytes accessed | tf_op | source)
XLA Modules:
  0.0 110.5 jit_solution(18032154906949071537)
XLA Ops:
  0.6 106.4 %shard_map.179 = (bf16[576,2304]{1,0:T(8,128)(2,1)S(1)}, bf16[576,2304]{1,0:T(8,128)(2,1)S(1)}, f32[576,576]{1,0:T(8,128)S(1)}, f32[576,576]{1,0:T(8,128)S(1)}, ...) custom-call(bf16[1024,2304]{1,0:T(8,128)(2,1)} %out_cot.1, ...), custom_call_target="tpu_custom_call" | custom-call | flops 10000000000 | bytes 30000000 | tf_op jit(solution)/shard_map/pallas_call | solution.py:453
  107.0 3.5 %shard_map.180 = (bf16[576,2304]{1,0:T(8,128)(2,1)}, bf16[576,2304]{1,0:T(8,128)(2,1)}, f32[576,576]{1,0:T(8,128)}, f32[576,576]{1,0:T(8,128)}, f32[48,576]{1,0:...) custom-call(bf16[576,2304]{1,0:T(8,128)(2,1)S(1)} %get-tuple-element.24.refs_0_, ...), custom_call_target="tpu_custom_call" | custom-call | flops 1000000 | bytes 20000000 | tf_op jit(solution)/shard_map/pallas_call | solution.py:492

commit v3 on v2

--- a/solution.py
+++ b/solution.py
@@ -71,8 +71,16 @@
     return index + bit - 2 * bit * lax.rem(index // bit, 2)
 
 
+def cut(total):
+    sizes = []
+    while total:
+        sizes.append(-(-total // 3))
+        total -= sizes[-1]
+    return sizes
+
+
 def main_kernel(
-    fs, tp, chunks, grad_bound,
+    fs, tp, sizes, grad_bound,
     out_cot, block_in, gated, gate, factor_out, factor_z, weight_out, weight_z,
     first_out, second_out, first_z, second_z,
     copy_out, copy_z, step_out, step_z, new_first_out, new_second_out, new_first_z, new_second_z,
@@ -87,32 +95,27 @@
     rank = factor_out.shape[0]
     share = rank // fs
     tokens = out_cot.shape[0]
-    rows = inner // chunks
+    chunks = len(sizes)
+    starts = [sum(sizes[:c]) for c in range(chunks)]
     entries = float(width * fs * inner * tp)
     part = lax.rem(mine, PARTS)
     piece = 2 * rank // PARTS
 
-    loads = []
-
-    def fetch(src, dst):
-        copy = pltpu.make_async_copy(src, dst, load.at[len(loads)])
-        copy.start()
-        loads.append(copy)
-        return copy
-
-    in_factor = [
-        fetch(factor_out, full.at[me, pl.ds(0, rank)]),
-        fetch(factor_z, full.at[me, pl.ds(rank, rank)]),
-    ]
-    in_weight = [fetch(weight_out, wo_v), fetch(weight_z, wz_v)]
-
     barrier = pltpu.get_barrier_semaphore()
     for d in range(1, fs):
         pl.semaphore_signal(barrier, inc=1, device_id={"fs": lax.rem(me + d, fs)}, device_id_type=MESH)
     for d in range(1, tp):
         pl.semaphore_signal(barrier, inc=1, device_id={"tp": lax.rem(mine + d, tp)}, device_id_type=MESH)
-    for copy in in_factor:
-        copy.wait()
+
+    def fetch(src, dst, k):
+        copy = pltpu.make_async_copy(src, dst, load.at[k])
+        copy.start()
+        return copy
+
+    fetch(factor_out, full.at[me, pl.ds(0, rank)], 0)
+    fetch(factor_z, full.at[me, pl.ds(rank, rank)], 0)
+    in_weight = [fetch(weight_out, wo_v, 1), fetch(weight_z, wz_v, 2)]
+    pltpu.make_async_copy(full.at[me], full.at[me], load.at[0]).wait()
     pl.semaphore_wait(barrier, fs + tp - 2)
 
     def piece_of(src, p):
@@ -128,92 +131,85 @@
     for copy in in_weight:
         copy.wait()
     in_tokens = [
-        (fetch(out_cot, tokens_v.at[0]), fetch(gated, inner_v.at[0])),
-        (fetch(block_in, tokens_v.at[1]), fetch(gate, inner_v.at[1])),
+        (fetch(out_cot, tokens_v.at[0], 3), fetch(gated, inner_v.at[0], 4)),
+        (fetch(block_in, tokens_v.at[1], 5), fetch(gate, inner_v.at[1], 6)),
     ]
-    in_moments = [
-        fetch(ref, moments_v.at[i]) for i, ref in enumerate((first_out, first_z, second_out, second_z))
-    ]
+    for i, ref in enumerate((first_out, first_z, second_out, second_z)):
+        fetch(ref, moments_v.at[i], 7)
     wt_v[...] = wz_v[...].T
 
     def chunk_of(src, c):
-        return wall.at[src, pl.ds(pl.multiple_of(c * rows, rows), rows)]
+        return wall.at[src, pl.ds(starts[c], sizes[c])]
 
     def up(h, c):
         block = chunk_of(jnp.maximum(me - h, 0), c)
-        return remote(block, block, send_u.at[h, c], recv_u.at[h, c], fs=jnp.minimum(me + 1, fs - 1))
+        return remote(block, block, send_u.at[h], recv_u.at[h, c], fs=jnp.minimum(me + 1, fs - 1))
 
     def down(h, c):
         block = chunk_of(jnp.minimum(me + h, fs - 1), c)
-        return remote(block, block, send_d.at[h, c], recv_d.at[h, c], fs=jnp.maximum(me - 1, 0))
-
-    def start_own(c):
-        @pl.when(me < fs - 1)
+        return remote(block, block, send_d.at[h], recv_d.at[h, c], fs=jnp.maximum(me - 1, 0))
+
+    late = lax.rem(mine, 2) == 1
+
+    def start_own(c, now):
+        @pl.when((me < fs - 1) & now)
         def _():
             up(0, c).start()
 
-        @pl.when(me > 0)
+        @pl.when((me > 0) & now)
         def _():
             down(0, c).start()
 
-    def pack(c, _):
-        at = pl.ds(pl.multiple_of(c * rows, rows), rows)
+    def pack(r, _):
+        at = pl.ds(pl.multiple_of(r * 16, 16), 16)
         pair = jnp.concatenate([wo_v[at, :], wt_v[at, :]], axis=1)
         wall[me, at, :] = encode(pair, WEIGHT_BOUND, 1)
-
-        @pl.when(c > 0)
-        def _():
-            start_own(c - 1)
-
         return 0
 
-    lax.fori_loop(0, chunks, pack, 0)
-    start_own(chunks - 1)
+    for c in range(chunks):
+        lax.fori_loop(starts[c] // 16, (starts[c] + sizes[c]) // 16, pack, 0)
+        if c:
+            start_own(c - 1, ~late)
+    start_own(chunks - 1, ~late)
 
     def pump(h, low, high, rising=True, falling=True):
-        def body(c, _):
+        for c in range(low, high):
             @pl.when((me - h >= 0) & (me < fs - 1) & rising)
-            def _():
+            def _(c=c):
                 up(h - 1, c).wait_recv()
                 up(h, c).start()
 
             @pl.when((me + h < fs) & (me > 0) & falling)
-            def _():
+            def _(c=c):
                 down(h - 1, c).wait_recv()
                 down(h, c).start()
 
-            return 0
-
-        lax.fori_loop(low, high, body, 0)
-
-    plane = []
-
-    def pass_on(d, k, p, bit):
+    def pass_on(d, p, bit, k):
         block = piece_of(lax.rem(me - d + fs, fs), p)
-        copy = remote(block, block, send_p.at[d - 1, k], recv_p.at[d - 1, k], tp=flip(mine, bit))
+        copy = remote(block, block, send_p.at[d - 1], recv_p.at[d - 1, k], tp=flip(mine, bit))
         copy.start()
-        plane.append(copy)
         return copy
 
     by_y, by_x = [], []
     for d in range(1, fs):
         spread[d - 1].wait_recv()
-        by_y.append(pass_on(d, 0, part, 4))
-        by_x.append([pass_on(d, 1, part, 2)])
-        pass_on(d, 3, part, 1)
+        by_y.append(pass_on(d, part, 4, 0))
+        by_x.append([pass_on(d, part, 2, 1)])
+        pass_on(d, part, 1, 3)
     for d in range(1, fs):
         by_y[d - 1].wait_recv()
-        by_x[d - 1].append(pass_on(d, 2, flip(part, 4), 2))
-        pass_on(d, 4, flip(part, 4), 1)
+        by_x[d - 1].append(pass_on(d, flip(part, 4), 2, 2))
+        pass_on(d, flip(part, 4), 1, 3)
+    for c in range(chunks):
+        start_own(c, late)
     for d in range(1, fs):
         for k, copy in enumerate(by_x[d - 1]):
             copy.wait_recv()
             p = flip(part, 2)
-            pass_on(d, 5 + k, p if k == 0 else flip(p, 4), 1)
-    waited = [c for c in by_y] + [c for pair in by_x for c in pair]
-    for copy in plane:
-        if not any(copy is other for other in waited):
-            copy.wait_recv()
+            pass_on(d, p if k == 0 else flip(p, 4), 1, 3)
+    for d in range(1, fs):
+        block = full.at[0, pl.ds(0, 4 * piece)]
+        remote(block, block, send_p.at[d - 1], recv_p.at[d - 1, 3], tp=flip(mine, 1)).wait_recv()
 
     block_t = 256 if tokens % 256 == 0 else tokens
     for m in range(2):
@@ -234,7 +230,7 @@
         term[m] = jnp.zeros((rank, inner), f32)
         lax.fori_loop(0, tokens // block_t, project, 0)
 
-    half = chunks // 2 + 1
+    half = 2
     upper = me * 2 >= fs
     lower = me * 2 < fs
     if fs > 2:
@@ -270,8 +266,7 @@
         t = fs - 1 - k
         link(t, me == 0, (me > 0) & (me < t), rise, rise_out, rise_in, t - 1)
         link(k, me == fs - 1, (me < fs - 1) & (me > k), fall, fall_out, fall_in, k)
-    for copy in in_moments:
-        copy.wait()
+    pltpu.make_async_copy(moments_v, moments_v, load.at[7]).wait()
     own = pl.ds(pl.multiple_of(me * share, share), share)
     sum_v[...] = jnp.concatenate([term[0, own, :], term[1, own, :]], axis=1)
 
@@ -295,20 +290,18 @@
     new_first_z[...] = moment[:, inner:]
     new_second_out[...] = square[:, :inner]
     new_second_z[...] = square[:, inner:]
-    gathers = []
     for d in range(1, fs):
         block = dir_code.at[me]
-        copy = remote(block, block, send_g.at[d - 1], recv_g.at[d - 1], fs=lax.rem(me + d, fs))
-        copy.start()
-        gathers.append(copy)
+        remote(block, block, send_g.at[0], recv_g.at[0], fs=lax.rem(me + d, fs)).start()
     if fs > 2:
         pump(1, half, chunks, upper, lower)
         pump(1, 0, chunks, lower, upper)
-    few = chunks // 6
+    few = 1
     if fs > 3:
         pump(2, 0, few)
-    for copy in gathers:
-        copy.wait_recv()
+    block = dir_code.at[pl.ds(0, fs - 1)]
+    gathers = remote(block, block, send_g.at[0], recv_g.at[0], fs=lax.rem(me + 1, fs))
+    gathers.wait_recv()
 
     whole = decode(jnp.concatenate([dir_code[s] for s in range(fs)], axis=0), DIR_BOUND, 3)
     for m in range(2):
@@ -335,13 +328,8 @@
     partial[...] = jnp.where(row == 0, squares[0], squares[1])
     own_z = full[me, pl.ds(rank, rank), :]
     step_z[...] = tn(own_z, dir_n[0]) + tn(own_z, dir_n[1])
-    totals = []
     for d in range(1, tp):
-        copy = remote(
-            partial, received.at[d - 1], send_t.at[d - 1], recv_t.at[d - 1], tp=lax.rem(mine + d, tp)
-        )
-        copy.start()
-        totals.append(copy)
+        remote(partial, received.at[d - 1], send_t.at[0], recv_t.at[0], tp=lax.rem(mine + d, tp)).start()
     own_out = full[me, pl.ds(0, rank), :]
     step_out[...] = nn(dir_t[0, 0], own_out) + nn(dir_t[0, 1], own_out)
     if fs > 3:
@@ -349,53 +337,36 @@
     for h in range(3, fs - 1):
         pump(h, 0, chunks)
     result = partial[...]
+    totals = remote(received, received, send_t.at[0], recv_t.at[0], tp=lax.rem(mine + 1, tp))
+    totals.wait_recv()
     for d in range(1, tp):
-        totals[d - 1].wait_recv()
         result = result + received[d - 1]
     scale = lax.rsqrt(result * (1.0 / entries) + norm_eps)
     scale_out, scale_z = scale[0:1, 0:1], scale[1:2, 0:1]
     step_out[...] = step_out[...] * scale_out
     step_z[...] = step_z[...] * scale_z
 
-    def finish(c, _):
-        @pl.when(me == fs - 1)
-        def _():
-            for h in range(fs - 1):
-                up(h, c).wait_recv()
-
-        @pl.when(me == 0)
-        def _():
-            for h in range(fs - 1):
-                down(h, c).wait_recv()
-
-        def fresh(r, _):
-            at = pl.ds(pl.multiple_of(c * rows + r * 16, 16), 16)
-            for m, (dst, size) in enumerate(((copy_out, scale_out), (copy_z, scale_z))):
-                code = jnp.concatenate(
-                    [wall[s, at, m * width:(m + 1) * width] for s in range(fs)], axis=1
-                )
-                step = update[m, at, :] * size
-                dst[at, :] = (decode(code, WEIGHT_BOUND, 1) - rate * step).astype(bf16)
-            return 0
-
-        lax.fori_loop(0, rows // 16, fresh, 0)
-        return 0
-
-    lax.fori_loop(0, chunks, finish, 0)
-
-    for h in range(fs - 1):
-        def drain(c, _, h=h):
-            @pl.when((me - h >= 0) & (me < fs - 1))
-            def _():
-                up(h, c).wait_send()
-
-            @pl.when((me + h < fs) & (me > 0))
-            def _():
-                down(h, c).wait_send()
-
-            return 0
-
-        lax.fori_loop(0, chunks, drain, 0)
+    def drain(ends):
+        for h in range(fs - 1):
+            @pl.when((me - h >= 0) & (me < fs - 1) & ends)
+            def _(h=h):
+                block = wall.at[0]
+                remote(block, block, send_u.at[h], recv_u.at[h, 0], fs=jnp.minimum(me + 1, fs - 1)).wait_send()
+
+            @pl.when((me + h < fs) & (me > 0) & ends)
+            def _(h=h):
+                block = wall.at[0]
+                remote(block, block, send_d.at[h], recv_d.at[h, 0], fs=jnp.maximum(me - 1, 0)).wait_send()
+
+    outer = (me == 0) | (me == fs - 1)
+    drain(outer)
+    block = full.at[0, pl.ds(0, (PARTS - 1) * piece)]
+    for d in range(1, fs):
+        remote(block, block, send_p.at[d - 1], recv_p.at[d - 1, 3], tp=flip(mine, 1)).wait_send()
+    for copy in spread:
+        copy.wait_send()
+    gathers.wait_send()
+    totals.wait_send()
     for k in range(fs - 1):
         t = fs - 1 - k
 
@@ -407,8 +378,30 @@
         def _(k=k):
             fall(k).wait_send()
 
-    for copy in spread + plane + gathers + totals:
-        copy.wait_send()
+    def fresh(r, _):
+        at = pl.ds(pl.multiple_of(r * 16, 16), 16)
+        for m, (dst, size) in enumerate(((copy_out, scale_out), (copy_z, scale_z))):
+            code = jnp.concatenate(
+                [wall[s, at, m * width:(m + 1) * width] for s in range(fs)], axis=1
+            )
+            step = update[m, at, :] * size
+            dst[at, :] = (decode(code, WEIGHT_BOUND, 1) - rate * step).astype(bf16)
+        return 0
+
+    for c in range(chunks):
+        @pl.when(me == fs - 1)
+        def _(c=c):
+            for h in range(fs - 1):
+                up(h, c).wait_recv()
+
+        @pl.when(me == 0)
+        def _(c=c):
+            for h in range(fs - 1):
+                down(h, c).wait_recv()
+
+        lax.fori_loop(starts[c] // 16, (starts[c] + sizes[c]) // 16, fresh, 0)
+
+    drain((me > 0) & (me < fs - 1))
 
 
 def store_kernel(*refs):
@@ -431,7 +424,8 @@
     width, rank = factor_out.shape
     tokens, inner = gated_out.shape
     share = rank // fs
-    chunks = next(n for n in (12, 6, 3, 2, 1) if inner % (16 * n) == 0)
+    sizes = [16 * n for n in cut(inner // 16)]
+    chunks = len(sizes)
     grad_bound = 2.0 ** math.ceil(
         math.log2(tokens * VALUE_BOUND * width * fs * VALUE_BOUND * FACTOR_BOUND)
     )
@@ -448,10 +442,10 @@
     hops = dma((fs - 1, chunks))
     peers = dma((fs - 1,))
     chain = dma((2, fs - 1))
-    others = dma((tp - 1,))
-    pieces = dma((fs - 1, PARTS - 1))
+    single = dma((1,))
+    pieces = dma((fs - 1, 4))
     made = pl.pallas_call(
-        functools.partial(main_kernel, fs, tp, chunks, grad_bound),
+        functools.partial(main_kernel, fs, tp, sizes, grad_bound),
         out_shape=tuple(pltpu.VMEM(r.shape, r.dtype) for r in results),
         in_specs=[ANY] * 12,
         out_specs=[VMEM] * 8,
@@ -477,9 +471,9 @@
             pltpu.VMEM((2, inner, fs * width), f32),
             pltpu.VMEM((8, 128), f32),
             pltpu.VMEM((tp - 1, 8, 128), f32),
-            dma((12,)),
-            peers, peers, pieces, pieces, hops, hops, hops, hops,
-            chain, chain, peers, peers, others, others,
+            dma((8,)),
+            peers, peers, peers, pieces, peers, hops, peers, hops,
+            chain, chain, single, single, single, single,
         ],
         compiler_params=pltpu.CompilerParams(
             collective_id=0, has_side_effects=True, vmem_limit_bytes=48 * 1024 * 1024

time: 113 us -> 110 us (0.973); the launches traced: 111 us -> 110 us
  no operation moved by 1% of the time
where the time goes in v3:
time: 110 us
  Pallas kernels  109 us (99%)
    pallas_call x1, Pallas kernels, per_device(): pl.pallas_call(functools.partial(main_kernel, fs, tp, sizes, grad_bound),...  106 us
    pallas_call x1, Pallas kernels, per_device(): pl.pallas_call(store_kernel, out_shape=results, in_specs=[VMEM] * 8, out_...  3.47 us

profile of v3, /device:TPU:1, one launch (start us, length us, event | category | flops | bytes accessed | tf_op | source)
XLA Modules:
  0.0 110.0 jit_solution(11797678975505172994)
XLA Ops:
  0.6 105.7 %shard_map.179 = (bf16[576,2304]{1,0:T(8,128)(2,1)S(1)}, bf16[576,2304]{1,0:T(8,128)(2,1)S(1)}, f32[576,576]{1,0:T(8,128)S(1)}, f32[576,576]{1,0:T(8,128)S(1)}, ...) custom-call(bf16[1024,2304]{1,0:T(8,128)(2,1)} %out_cot.1, ...), custom_call_target="tpu_custom_call" | custom-call | flops 10000000000 | bytes 30000000 | tf_op jit(solution)/shard_map/pallas_call | solution.py:447
  106.4 3.5 %shard_map.180 = (bf16[576,2304]{1,0:T(8,128)(2,1)}, bf16[576,2304]{1,0:T(8,128)(2,1)}, f32[576,576]{1,0:T(8,128)}, f32[576,576]{1,0:T(8,128)}, f32[48,576]{1,0:...) custom-call(bf16[576,2304]{1,0:T(8,128)(2,1)S(1)} %get-tuple-element.24.refs_0_, ...), custom_call_target="tpu_custom_call" | custom-call | flops 1000000 | bytes 20000000 | tf_op jit(solution)/shard_map/pallas_call | solution.py:486
